TPU v7x, 32 devices: a whole 2x2x4 slice. The times are simulated.
32 devices in a mesh: sp: 4 (over z), fs: 4 (over y, x), tp: 2 (over core).
Axes of the slice: x: 2, y: 2, z: 4, core: 2. Of those that a mesh axis runs over, the one named last changes fastest.
Arguments:
- tokens: bfloat16 [4, 512, 2048], P('fs', ('sp', 'tp')), may hold values from -6 to 6
- norm_gain: float32 [2048], replicated, may hold values from 0.1 to 1.9
- rec_query: bfloat16 [2048, 512], P('sp', 'tp'), may hold values from -0.125 to 0.125
- rec_input: bfloat16 [2048, 512], P('sp', 'tp'), may hold values from -0.125 to 0.125
- rec_forward: bfloat16 [2048, 512], P('sp', 'tp'), may hold values from -0.125 to 0.125
- rec_backward: bfloat16 [2048, 512], P('sp', 'tp'), may hold values from -0.125 to 0.125
- forget_gap: float32 [2, 512], P(None, 'tp'), may hold values from 0 to 0.06
- log_decay: float32 [4, 2, 4, 512], P('fs', None, 'tp', 'sp'), may hold values from -0.7 to 0
- rec_gain: float32 [512], P('tp'), may hold values from 0.1 to 1.9
- conv_value: bfloat16 [2048, 512], P('sp', 'tp'), may hold values from -0.125 to 0.125
- conv_gate: bfloat16 [2048, 512], P('sp', 'tp'), may hold values from -0.125 to 0.125
- conv_kernel: bfloat16 [31, 512], P(None, 'tp'), may hold values from -3.1 to 3.1
- conv_gain: float32 [512], P('tp'), may hold values from 0.1 to 1.9
- out_rec: bfloat16 [512, 2048], P('tp', 'sp'), may hold values from -0.1875 to 0.1875
- out_conv: bfloat16 [512, 2048], P('tp', 'sp'), may hold values from -0.1875 to 0.1875
Outputs:
- mixed: bfloat16 [4, 512, 2048], P('fs', ('sp', 'tp'))
All inputs are finite; a program needn't handle non-finite values.
Results may differ from a plain program's by a relative error of at most 0.017.
Values may be sent and summed in bfloat16 or wider, within the bound.
A program may use at most 64 MiB of HBM per device.

v0:
```python
import jax
import jax.numpy as jnp
from jax import lax
from jax.sharding import PartitionSpec as P

KD = 128
VD = 128
BLOCK = 64


EPS = 1e-06
HIGH = lax.Precision.HIGHEST


def entering(x, axis, join, neutral, backward):
    count = lax.axis_size(axis)
    place = lax.axis_index(axis)
    ahead = count - 1 - place if backward else place
    gathered = jax.tree.map(
        lambda a, kind: lax.all_gather(a.astype(kind), axis), x, (jnp.bfloat16, jnp.bfloat16)
    )
    state = jax.tree.map(lambda a, e: jnp.zeros_like(a) + jnp.asarray(e, a.dtype), x, neutral)

    def one(lap, state):
        source = count - 1 - lap if backward else lap
        return join(
            state,
            jax.tree.map(
                lambda a, own: lax.dynamic_index_in_dim(a, source, 0, False).astype(own.dtype),
                gathered,
                x,
            ),
        )

    return lax.fori_loop(0, ahead, one, state)


def padded_2(cells, sides, width):
    for axis, dim in sides:
        count = lax.axis_size(axis)
        ends = count - 1
        head = lax.slice_in_dim(cells, 0, width, axis=dim)
        tail = lax.slice_in_dim(cells, cells.shape[dim] - width, cells.shape[dim], axis=dim)
        cells = jnp.concatenate(
            [
                lax.ppermute(tail, axis, [(i, (i + 1) % count) for i in range(ends)]),
                cells,
                lax.ppermute(head, axis, [((i + 1) % count, i) for i in range(ends)]),
            ],
            axis=dim,
        )
    return cells


def block_pass(queries, key_rows, value_rows, log_gate):
    heads_n, length_n, key_dim = queries.shape
    value_dim = value_rows.shape[-1]
    blocks = length_n // BLOCK

    def split_blocks(tensor):
        return tensor.reshape(heads_n, blocks, BLOCK, tensor.shape[-1]).transpose(1, 0, 2, 3)

    def join_blocks(tensor):
        return tensor.transpose(1, 0, 2, 3).reshape(heads_n, length_n, tensor.shape[-1])

    lower_mask = jnp.tril(jnp.ones((BLOCK, BLOCK), bool))

    def advance(carried, inputs):
        states, offset = carried
        query_b, key_b, value_b, gate_b = inputs
        cumulative = jnp.cumsum(gate_b, axis=1)
        query_g = query_b * jnp.exp(cumulative)
        key_g = key_b * jnp.exp(-cumulative)
        scores = jnp.einsum("htd,hsd->hts", query_g, key_g, precision=HIGH)
        scores = jnp.where(lower_mask, scores, 0.0)
        result = jnp.einsum("hts,hse->hte", scores, value_b, precision=HIGH)
        result = result + jnp.einsum("htd,hde->hte", query_g, states, precision=HIGH)
        last_g = cumulative[:, -1, :]
        weighted = key_b * jnp.exp(last_g[:, None, :] - cumulative)
        states = jnp.exp(last_g)[:, :, None] * states + jnp.einsum(
            "hsd,hse->hde", weighted, value_b, precision=HIGH
        )
        decayed = query_b * jnp.exp(offset[:, None, :] + cumulative)
        return ((states, offset + last_g), (result, decayed))

    start_state = jnp.zeros((heads_n, key_dim, value_dim), jnp.float32)
    start_offset = jnp.zeros((heads_n, key_dim), jnp.float32)
    inputs = (
        split_blocks(queries),
        split_blocks(key_rows),
        split_blocks(value_rows),
        split_blocks(log_gate),
    )
    final_pair, outputs = lax.scan(advance, (start_state, start_offset), inputs)
    return (join_blocks(outputs[0]), join_blocks(outputs[1]), final_pair[1], final_pair[0])


def chain_combine(first_part, second_part):
    return (
        first_part[0] * second_part[0],
        second_part[0][:, :, None] * first_part[1] + second_part[1],
    )


def recurrence(query_pre, input_pre, forward_pre, backward_pre, forget_gap, log_decay, rec_gain):
    heads_local = log_decay.shape[2]
    row_count = query_pre.shape[0]

    def to_heads(tensor):
        return tensor.astype(jnp.float32).reshape(row_count, heads_local, -1).transpose(1, 0, 2)

    def gate_terms(pre_act, gap_row, decay_row):
        closing = jax.nn.sigmoid(-to_heads(pre_act)) * gap_row.reshape(heads_local, 1, -1)
        return (closing, jnp.log1p(-closing) + decay_row[:, :, None])

    queries = jax.nn.silu(to_heads(query_pre)) * KD ** (-0.5)
    values = to_heads(input_pre)
    keys_fwd, gate_fwd = gate_terms(forward_pre, forget_gap[0], log_decay[0, 0])
    keys_bwd, gate_bwd = gate_terms(backward_pre, forget_gap[1], log_decay[0, 1])
    identity = (
        jnp.ones((heads_local, KD), jnp.float32),
        jnp.zeros((heads_local, KD, VD), jnp.float32),
    )
    local_fwd, decayed_fwd, offset_fwd, state_fwd = block_pass(queries, keys_fwd, values, gate_fwd)
    incoming_fwd = entering((jnp.exp(offset_fwd), state_fwd), "sp", chain_combine, identity, False)
    forward = local_fwd + jnp.einsum("htd,hde->hte", decayed_fwd, incoming_fwd[1], precision=HIGH)
    local_bwd, decayed_bwd, offset_bwd, state_bwd = block_pass(
        jnp.flip(queries, 1), jnp.flip(keys_bwd, 1), jnp.flip(values, 1), jnp.flip(gate_bwd, 1)
    )
    incoming_bwd = entering((jnp.exp(offset_bwd), state_bwd), "sp", chain_combine, identity, True)
    backward = jnp.flip(
        local_bwd + jnp.einsum("htd,hde->hte", decayed_bwd, incoming_bwd[1], precision=HIGH), 1
    )
    joined = forward + backward
    joined = joined * lax.rsqrt(jnp.mean(joined * joined, axis=-1, keepdims=True) + EPS)
    joined = joined * rec_gain.reshape(heads_local, 1, VD)
    return joined.transpose(1, 0, 2).reshape(row_count, heads_local * VD).astype(jnp.bfloat16)


def convolve(conv_pre, glu_pre, conv_kernel, conv_gain):
    gated = (conv_pre.astype(jnp.float32) * jax.nn.sigmoid(glu_pre.astype(jnp.float32))).astype(
        jnp.bfloat16
    )
    half_width = conv_kernel.shape[0] // 2
    padded = padded_2(gated, (("sp", 0),), half_width)
    convolved = lax.conv_general_dilated(
        padded.astype(jnp.float32)[None],
        conv_kernel.astype(jnp.float32)[:, None, :],
        (1,),
        "VALID",
        dimension_numbers=("NWC", "WIO", "NWC"),
        feature_group_count=gated.shape[1],
        precision=HIGH,
    )[0]
    totals = lax.psum((jnp.sum(convolved, axis=-1), jnp.sum(convolved * convolved, axis=-1)), "tp")
    full_width = convolved.shape[1] * lax.axis_size("tp")
    mean_c = (totals[0] / full_width)[:, None]
    variance = (totals[1] / full_width)[:, None] - mean_c * mean_c
    return jax.nn.silu((convolved - mean_c) * lax.rsqrt(variance + EPS) * conv_gain).astype(
        jnp.bfloat16
    )


def body(
    tokens,
    norm_gain,
    rec_query,
    rec_input,
    rec_forward,
    rec_backward,
    forget_gap,
    log_decay,
    rec_gain,
    conv_value,
    conv_gate,
    conv_kernel,
    conv_gain,
    out_rec,
    out_conv,
):
    row_values = tokens[0].astype(jnp.float32)
    normed = row_values * lax.rsqrt(jnp.mean(row_values * row_values, axis=-1, keepdims=True) + EPS)
    normed = (normed * norm_gain).astype(jnp.bfloat16)
    whole = lax.all_gather(normed, "tp", axis=0, tiled=True)
    row_count = whole.shape[0]
    pieces = (
        lax.all_gather(rec_query, "sp", axis=0, tiled=True),
        lax.all_gather(rec_input, "sp", axis=0, tiled=True),
        lax.all_gather(rec_forward, "sp", axis=0, tiled=True),
        lax.all_gather(rec_backward, "sp", axis=0, tiled=True),
        lax.all_gather(conv_value, "sp", axis=0, tiled=True),
        lax.all_gather(conv_gate, "sp", axis=0, tiled=True),
    )
    results = tuple(
        (
            jnp.dot(whole, weight_piece, preferred_element_type=jnp.float32)
            for weight_piece in pieces
        )
    )
    projected = tuple((result.astype(jnp.bfloat16) for result in results))
    rec_out = recurrence(
        projected[0], projected[1], projected[2], projected[3], forget_gap, log_decay, rec_gain
    )
    conv_out = convolve(projected[4], projected[5], conv_kernel, conv_gain)
    both_out = jnp.concatenate([rec_out, conv_out], axis=1)
    out_local = jnp.concatenate([out_rec, out_conv], axis=0)
    full_columns = lax.all_gather(out_local, "sp", axis=1, tiled=True)
    own_rows = row_count // lax.axis_size("tp")
    rows_part = lax.slice_in_dim(both_out, 0, own_rows * lax.axis_size("tp"), axis=0)
    mixed = lax.psum_scatter(
        jnp.dot(rows_part, full_columns, preferred_element_type=jnp.float32).astype(jnp.bfloat16),
        "tp",
        scatter_dimension=0,
        tiled=True,
    )
    return mixed[None]


def solution(mesh):
    return jax.shard_map(
        body,
        mesh=mesh,
        in_specs=(
            P("fs", ("sp", "tp"), None),
            P(),
            P("sp", "tp"),
            P("sp", "tp"),
            P("sp", "tp"),
            P("sp", "tp"),
            P(None, "tp"),
            P("fs", None, "tp", "sp"),
            P("tp"),
            P("sp", "tp"),
            P("sp", "tp"),
            P(None, "tp"),
            P("tp"),
            P("tp", "sp"),
            P("tp", "sp"),
        ),
        out_specs=P("fs", ("sp", "tp"), None),
        check_vma=False,
    )
```

profile of v0, /device:TPU:0, one launch (start us, length us, event | category | flops | bytes accessed | tf_op | source)
XLA Modules:
  0.0 254.0 jit_solution(9676537296422704359)
XLA Ops:
  6.5 0.7 all-gather.20.cloned.1.call-update
  7.3 0.7 all-gather.14.cloned.1.call-update
  8.1 0.7 all-gather.18.cloned.1.call-update
  8.8 0.5 all-gather.16.cloned.1.call-update
  9.4 0.5 all-gather.22.cloned.1.call-update
  10.0 0.5 all-gather.24.cloned.1.call-update
  10.6 1.9 pad_maximum_fusion
  12.9 2.3 all_gather.48
  15.2 24.4 %all-gather.20.cloned.1.call-done = bf16[2048,256]{1,0:T(8,128)(2,1)} async-done(((bf16[512,256]{1,0:T(8,128)(2,1)}), bf16[2048,256]{1,0:T(8,128)(2,1)}) %all-gather.20.cloned.1.call-update) | async-done | bytes 1048592 | tf_op jit(solution)/shard_map/all_gather | solution.py:190
  39.6 1.5 fusion.63
  41.2 27.4 %all-gather.14.cloned.1.call-done = bf16[2048,256]{1,0:T(8,128)(2,1)} async-done(((bf16[512,256]{1,0:T(8,128)(2,1)}), bf16[2048,256]{1,0:T(8,128)(2,1)}) %all-gather.14.cloned.1.call-update) | async-done | bytes 1048592 | tf_op jit(solution)/shard_map/all_gather | solution.py:189
  68.6 1.5 fusion.72
  70.5 27.1 %all-gather.18.cloned.1.call-done = bf16[2048,256]{1,0:T(8,128)(2,1)} async-done(((bf16[512,256]{1,0:T(8,128)(2,1)}), bf16[2048,256]{1,0:T(8,128)(2,1)}) %all-gather.18.cloned.1.call-update) | async-done | bytes 1048592 | tf_op jit(solution)/shard_map/all_gather | solution.py:187
  97.6 1.5 fusion.65
  99.3 27.1 %all-gather.16.cloned.1.call-done = bf16[2048,256]{1,0:T(8,128)(2,1)} async-done(((bf16[512,256]{1,0:T(8,128)(2,1)}), bf16[2048,256]{1,0:T(8,128)(2,1)}) %all-gather.16.cloned.1.call-update) | async-done | bytes 1048592 | tf_op jit(solution)/shard_map/all_gather | solution.py:188
  126.4 1.5 fusion.67
  128.1 2.7 %while.63 = (s32[]{:T(128)}, f32[2,128,128]{2,1,0:T(8,128)S(1)}, f32[2,128]{1,0:T(2,128)S(1)}, f32[2,2,64,128]{3,2,0,1:T(8,128)S(1)}, f32[2,2,64,128]{3,2,0,1:T(...) while((s32[]{:T(128)}, f32[2,128,128]{2,1,0:T(8,128)S(1)}, ...), condition=%wide.region_8.9_spmd.clone, body=%wide.region_6.8_spmd.clone.sunk | while | flops 76820992 | bytes 1827985 | solution.py:94
  130.8 16.3 %all-gather.3 = bf16[8,128,128]{2,1,0:T(8,128)(2,1)S(1)} all-gather(bf16[2,128,128]{2,1,0:T(8,128)(2,1)S(1)} %convert_element_type.127), channel_id=5, replica_groups=mesh['sp'=4,'fs'=4,'tp'=2] {'sp'}, dimensions={0}, use_global_device_ids=true | all-gather | bytes 327680 | tf_op jit(solution)/shard_map/all_gather | solution.py:20
  147.1 9.3 %all-gather.5 = bf16[4,2,128]{2,1,0:T(2,128)(2,1)S(1)} all-gather(bf16[1,2,128]{2,1,0:T(2,128)(2,1)S(1)} %fusion.94), channel_id=4, replica_groups=mesh['sp'=4,'fs'=4,'tp'=2] {'sp'}, dimensions={0}, use_global_device_ids=true | all-gather | bytes 2560 | tf_op jit(solution)/shard_map/all_gather | solution.py:20
  157.0 2.7 %while.62 = (s32[]{:T(128)}, f32[2,128,128]{2,1,0:T(8,128)S(1)}, f32[2,128]{1,0:T(2,128)S(1)}, f32[2,2,64,128]{3,2,0,1:T(8,128)S(1)}, f32[2,2,64,128]{3,2,0,1:T(...) while((s32[]{:T(128)}, f32[2,128,128]{2,1,0:T(8,128)S(1)}, ...), condition=%wide.region_3.4_spmd.clone, body=%wide.region_1.3_spmd.clone.sunk | while | flops 76820992 | bytes 1827985 | solution.py:94
  159.8 1.5 fusion.58
  161.3 25.3 %all-gather.24.cloned.1.call-done = bf16[2048,256]{1,0:T(8,128)(2,1)} async-done(((bf16[512,256]{1,0:T(8,128)(2,1)}), bf16[2048,256]{1,0:T(8,128)(2,1)}) %all-gather.24.cloned.1.call-update) | async-done | bytes 1048592 | tf_op jit(solution)/shard_map/all_gather | solution.py:192
  186.6 1.5 fusion.57
  188.9 3.4 %collective-permute-start = (bf16[15,256]{1,0:T(8,128)(2,1)S(1)}, bf16[15,256]{1,0:T(8,128)(2,1)S(1)}, u32[]{:S(2)}, u32[]{:S(2)}) collective-permute-start(bf16[15,256]{1,0:T(8,128)(2,1)S(1)} %get-tuple-element.425), channel_id=1, source_target_pairs={{0,8},{8,16},{16,24},{1,9},{9,17},{17,25},{2,10},{10,18},{18,26},{... | collective-permute-start | bytes 23048 | tf_op jit(solution)/shard_map/ppermute | solution.py:46
  192.3 1.3 collective-permute-start.1
  193.6 11.0 %all-gather.4 = bf16[4,2,128]{2,1,0:T(2,128)(2,1)S(1)} all-gather(bf16[1,2,128]{2,1,0:T(2,128)(2,1)S(1)} %fusion.93), channel_id=2, replica_groups=mesh['sp'=4,'fs'=4,'tp'=2] {'sp'}, dimensions={0}, use_global_device_ids=true | all-gather | bytes 2560 | tf_op jit(solution)/shard_map/all_gather | solution.py:20
  204.5 15.8 %all-gather.1 = bf16[8,128,128]{2,1,0:T(8,128)(2,1)S(1)} all-gather(bf16[2,128,128]{2,1,0:T(8,128)(2,1)S(1)} %convert_element_type.123), channel_id=3, replica_groups=mesh['sp'=4,'fs'=4,'tp'=2] {'sp'}, dimensions={0}, use_global_device_ids=true | all-gather | bytes 327680 | tf_op jit(solution)/shard_map/all_gather | solution.py:20
  221.1 2.2 fusion.102
  223.4 2.5 all-reduce
  226.0 11.4 %all-gather.26.cloned.1.call-done = bf16[512,2048]{1,0:T(8,128)(2,1)} async-done(((bf16[512,512]{1,0:T(8,128)(2,1)}), bf16[512,2048]{1,0:T(8,128)(2,1)}) %all-gather.26.cloned.1.call-update) | async-done | bytes 2097168 | tf_op jit(solution)/shard_map/all_gather | solution.py:207
  237.5 2.8 %convolution_convert_fusion = bf16[128,2048]{1,0:T(8,128)(2,1)} fusion(bf16[512,2048]{1,0:T(8,128)(2,1)} %all-gather.26.cloned.1.call-done, bf16[128,256]{1,0:T(8,128)(2,1)S(1)} %multiply_convert_fusion, bf16[128,256]{1,0:T(8,128)(2,1)S(1)} %copy.73), kind=kOutput, calls=%fused_computation.76 | convolution fusion | flops 268959744 | bytes 2752512 | tf_op jit(solution)/shard_map/dot_general | solution.py:211
  240.3 6.9 %reduce-scatter.2.cloned.1.call-done = bf16[64,2048]{1,0:T(8,128)(2,1)} async-done(((bf16[128,2048]{1,0:T(8,128)(2,1)}), bf16[64,2048]{1,0:T(8,128)(2,1)}) %reduce-scatter.2.cloned.1.call-update) | async-done | bytes 262160 | tf_op jit(solution)/shard_map/reduce_scatter | solution.py:210
  (115 shorter events, 9.0 us)
Async XLA Ops:
  6.5 214.6 %copy-start = (bf16[31,256]{1,0:T(8,128)(2,1)S(1)}, bf16[31,256]{1,0:T(8,128)(2,1)}, u32[]{:S(2)}) copy-start(bf16[31,256]{1,0:T(8,128)(2,1)} %param.34) | copy-start | bytes 47620
  6.5 6.1 %copy-start.1 = (bf16[1,64,2048]{2,1,0:T(8,128)(2,1)S(1)}, bf16[1,64,2048]{2,1,0:T(8,128)(2,1)}, u32[]{:S(2)}) copy-start(bf16[1,64,2048]{2,1,0:T(8,128)(2,1)} %param.23) | copy-start | bytes 786436
  6.5 6.2 %copy-start.2 = (f32[2048]{0:T(1024)S(1)}, f32[2048]{0:T(1024)}, u32[]{:S(2)}) copy-start(f32[2048]{0:T(1024)} %param.24) | copy-start | bytes 24580
  6.5 33.1 %all-gather.20.cloned.1.call-start = ((), (), s32[]{:S(2)}) async-start(), calls=%async_computation.4 | async-start | bytes 1310720 | tf_op jit(solution)/shard_map/all_gather | solution.py:190
  7.3 61.3 %all-gather.14.cloned.1.call-start = ((), (), s32[]{:S(2)}) async-start(), calls=%async_computation.1 | async-start | bytes 1310720 | tf_op jit(solution)/shard_map/all_gather | solution.py:189
  8.0 7.2 %copy-start.3 = (f32[2,256]{1,0:T(2,128)S(1)}, f32[2,256]{1,0:T(2,128)}, u32[]{:S(2)}) copy-start(f32[2,256]{1,0:T(2,128)} %param.29) | copy-start | bytes 6148
  8.0 7.2 %copy-start.4 = (f32[1,2,2,128]{3,2,1,0:T(2,128)S(1)}, f32[1,2,2,128]{3,2,1,0:T(2,128)}, u32[]{:S(2)}) copy-start(f32[1,2,2,128]{3,2,1,0:T(2,128)} %param.30) | copy-start | bytes 6148
  8.0 89.5 %all-gather.18.cloned.1.call-start = ((), (), s32[]{:S(2)}) async-start(), calls=%async_computation.3 | async-start | bytes 1310720 | tf_op jit(solution)/shard_map/all_gather | solution.py:187
  8.8 117.6 %all-gather.16.cloned.1.call-start = ((), (), s32[]{:S(2)}) async-start(), calls=%async_computation.2 | async-start | bytes 1310720 | tf_op jit(solution)/shard_map/all_gather | solution.py:188
  9.3 150.4 %all-gather.22.cloned.1.call-start = ((), (), s32[]{:S(2)}) async-start(), calls=%async_computation.5 | async-start | bytes 1310720 | tf_op jit(solution)/shard_map/all_gather | solution.py:191
  9.9 176.7 %all-gather.24.cloned.1.call-start = ((), (), s32[]{:S(2)}) async-start(), calls=%async_computation.6 | async-start | bytes 1310720 | tf_op jit(solution)/shard_map/all_gather | solution.py:192
  10.5 226.9 %all-gather.26.cloned.1.call-start = ((), (), s32[]{:S(2)}) async-start(), calls=%async_computation.7 | async-start | bytes 2621440 | tf_op jit(solution)/shard_map/all_gather | solution.py:207
  12.5 234.7 %reduce-scatter.2.cloned.1.call-start = ((), (), s32[]{:S(2)}) async-start(), calls=%async_computation.8 | async-start | bytes 786432 | tf_op jit(solution)/shard_map/reduce_scatter | solution.py:210
  188.2 32.7 %copy-start.5 = (f32[256]{0:T(256)S(1)}, f32[256]{0:T(256)}, u32[]{:S(2)}) copy-start(f32[256]{0:T(256)} %param.31) | copy-start | bytes 3076
  188.9 32.2 %collective-permute-start = (bf16[15,256]{1,0:T(8,128)(2,1)S(1)}, bf16[15,256]{1,0:T(8,128)(2,1)S(1)}, u32[]{:S(2)}, u32[]{:S(2)}) collective-permute-start(bf16[15,256]{1,0:T(8,128)(2,1)S(1)} %get-tuple-element.425), channel_id=1, source_target_pairs={{0,8},{8,16},{16,24},{1,9},{9,17},{17,25},{2,10},{10,18},{18,26},{... | collective-permute-start | bytes 23048 | tf_op jit(solution)/shard_map/ppermute | solution.py:46
  192.3 28.8 %collective-permute-start.1 = (bf16[15,256]{1,0:T(8,128)(2,1)S(1)}, bf16[15,256]{1,0:T(8,128)(2,1)S(1)}, u32[]{:S(2)}, u32[]{:S(2)}) collective-permute-start(bf16[15,256]{1,0:T(8,128)(2,1)S(1)} %get-tuple-element.426), channel_id=1, source_target_pairs={{8,0},{16,8},{24,16},{9,1},{17,9},{25,17},{10,2},{18,10},{26,18},{... | collective-permute-start | bytes 23048 | tf_op jit(solution)/shard_map/ppermute | solution.py:48
  220.4 5.5 %copy-start.6 = (f32[256]{0:T(256)S(1)}, f32[256]{0:T(256)}, u32[]{:S(2)}) copy-start(f32[256]{0:T(256)} %param.35) | copy-start | bytes 3076
Sparse Core Ops, SparseCore 0:
  8.9 30.6 all-gather.19
  41.2 27.3 all-gather.13
  70.2 27.3 all-gather.17
  99.0 27.3 all-gather.15
  127.8 30.0 all-gather.21
  159.3 27.2 all-gather.23
  188.2 49.2 all-gather.25
  240.4 6.7 reduce-scatter.1
where the time goes:
time: 255 us; the launch traced here: 254 us
  waiting for transfers between devices  153 us (60%)
  blocking collectives  57.2 us (22%)
  matrix products  19.5 us (8%)
  between operations  13.9 us (5%)
  starting transfers between devices  4.92 us (2%)
  other arithmetic  3.83 us (2%)
    all_gather x4, blocking collectives, entering(): lax.all_gather(a.astype(kind), axis)  52.4 us
    all_gather x1, waiting for transfers between devices, body(): lax.all_gather(rec_forward, 'sp', axis=0, tiled=True)  27.4 us
    all_gather x1, waiting for transfers between devices, body(): lax.all_gather(rec_input, 'sp', axis=0, tiled=True)  27.1 us
    all_gather x1, waiting for transfers between devices, body(): lax.all_gather(rec_query, 'sp', axis=0, tiled=True)  27.1 us
    all_gather x1, waiting for transfers between devices, body(): lax.all_gather(conv_gate, 'sp', axis=0, tiled=True)  25.3 us
    all_gather x1, waiting for transfers between devices, body(): lax.all_gather(rec_backward, 'sp', axis=0, tiled=True)  24.4 us
    all_gather x1, waiting for transfers between devices, body(): full_columns = lax.all_gather(out_local, 'sp', axis=1, tiled=True)  11.4 us
    dot_general x6, matrix products, body(): jnp.dot(whole, weight_piece, preferred_element_type=jnp.float32)  9.23 us
  transfers between devices with their start and end apart: 10, of which 7 were waited for; matrix products, arithmetic and copies ran while one was open for 8% of the time, Pallas kernels for 0%

commit v1 on v0

--- a/solution.py
+++ b/solution.py
@@ -1,6 +1,10 @@
+import functools
+
 import jax
 import jax.numpy as jnp
 from jax import lax
+from jax.experimental import pallas as pl
+from jax.experimental.pallas import tpu as pltpu
 from jax.sharding import PartitionSpec as P
 
 KD = 128
@@ -216,7 +220,508 @@
     return mixed[None]
 
 
+MESH = pl.DeviceIdType.MESH
+PACK = 8
+
+
+def dot_as(a, b, ca, cb, precision=HIGH):
+    return lax.dot_general(
+        a, b, (((ca,), (cb,)), ((), ())), precision=precision, preferred_element_type=jnp.float32
+    )
+
+
+def fused_kernel(
+    n, nf, hl, tokens, gain, w0, w1, w2, w3, w4, w5, pack, out_r, out_c, o_ref,
+    x, wbuf, ow, pk, ld, dec, proj, accf, accb, gp, yout, yall, mo, fin, st,
+    w_send, w_recv, x_send, x_recv, t_send, t_recv, d_send, p_send, p_recv, l_send, l_recv,
+    o_send, o_recv, a_send, a_recv, f_send, f_recv, s_send, s_recv, loc,
+):
+    s = lax.axis_index("sp")
+    f = lax.axis_index("fs")
+    t = lax.axis_index("tp")
+    other = 1 - t
+    rows = tokens.shape[1]
+    width = KD
+    weights = (w0, w1, w2, w3, w4, w5)
+    kslice = w0.shape[0]
+    krows = kslice // nf
+    half = out_r.shape[0]
+    groups = n * width
+
+    def at(sp=s, fs=f, tp=t):
+        return {"sp": sp, "fs": fs, "tp": tp}
+
+    def remote(src, dst, send, recv, to):
+        return pltpu.make_async_remote_copy(
+            src_ref=src, dst_ref=dst, send_sem=send, recv_sem=recv, device_id=to,
+            device_id_type=MESH,
+        )
+
+    barrier = pltpu.get_barrier_semaphore()
+    for d in range(n):
+        for c in range(2):
+            if d or c:
+                pl.semaphore_signal(
+                    barrier, inc=1, device_id=at(sp=lax.rem(s + d, n), tp=lax.rem(t + c, 2)),
+                    device_id_type=MESH,
+                )
+    for d in range(1, nf):
+        pl.semaphore_signal(
+            barrier, inc=1, device_id=at(fs=lax.rem(f + d, nf)), device_id_type=MESH
+        )
+    pl.semaphore_wait(barrier, 2 * n - 1 + nf - 1)
+
+    def wrows(place, quarter):
+        return pl.ds(pl.multiple_of(place * kslice + quarter * krows, krows), krows)
+
+    def wcols(core):
+        return pl.ds(0, (4 - 2 * core) * width)
+
+    mine = pl.ds(pl.multiple_of(f * krows, krows), krows)
+    for j in range(hl):
+        to_s = t * hl + j
+        cols = pl.ds(j * width, width)
+        for core in range(2):
+            here = (to_s == s) & (t == core)
+            for at_m, m in enumerate((0, 1, 2, 3) if core == 0 else (4, 5)):
+                src = weights[m].at[mine, cols]
+                dst = wbuf.at[wrows(s, f), pl.ds(at_m * width, width)]
+
+                @pl.when(here)
+                def _(src=src, dst=dst):
+                    pltpu.make_async_copy(src, dst, w_recv.at[s]).start()
+
+                @pl.when(jnp.logical_not(here))
+                def _(src=src, dst=dst, core=core, to_s=to_s):
+                    remote(
+                        src, dst, w_send.at[j, core], w_recv.at[s], at(sp=to_s, tp=core)
+                    ).start()
+
+        here0 = (to_s == s) & (t == 0)
+        src = pack.at[j, pl.ds(0, PACK)]
+
+        @pl.when(here0)
+        def _(src=src):
+            pltpu.make_async_copy(src, ld.at[s], l_recv.at[s]).start()
+
+        @pl.when(jnp.logical_not(here0))
+        def _(src=src, j=j, to_s=to_s):
+            remote(src, ld.at[s], l_send.at[j], l_recv.at[s], at(sp=to_s, tp=0)).start()
+
+        @pl.when(to_s == s)
+        def _(j=j):
+            pltpu.make_async_copy(pack.at[j], pk, p_recv).start()
+            remote(pack.at[j], pk, p_send, p_recv, at(tp=other)).start()
+
+    values = tokens[0].astype(jnp.float32)
+    normed = values * lax.rsqrt(jnp.mean(values * values, axis=-1, keepdims=True) + EPS)
+
+    def slot(place, core):
+        return pl.ds(pl.multiple_of(place * 2 * rows + core * rows, rows), rows)
+
+    x[slot(s, t), :] = (normed * gain[...]).astype(jnp.bfloat16)
+
+    def token(place, core, send, to):
+        part = x.at[slot(place, core)]
+        return remote(part, part, send, t_recv.at[place, core], to)
+
+    def token_right(place):
+        return token(place, t, t_send.at[place, 0], at(sp=lax.rem(s + 1, n)))
+
+    def token_left(place):
+        return token(place, t, t_send.at[place, 1], at(sp=lax.rem(s + n - 1, n)))
+
+    def token_partner(place):
+        return token(place, t, d_send.at[place], at(tp=other))
+
+    @pl.when(s < n - 1)
+    def _():
+        token_right(s).start()
+
+    @pl.when(s > 0)
+    def _():
+        token_left(s).start()
+
+    token_partner(s).start()
+
+    own_out = []
+    for which, ref in enumerate((out_r, out_c)):
+        part = ow.at[pl.ds(pl.multiple_of(which * groups + t * half, half), half)]
+        own_out.append(remote(ref, part, o_send.at[which], o_recv.at[which], at(tp=other)))
+        own_out[-1].start()
+        pltpu.make_async_copy(ref, part, loc.at[which]).start()
+
+    def share(core, place, d):
+        part = wbuf.at[wrows(place, f), wcols(core)]
+        return remote(
+            part, part, x_send.at[place, d], x_recv.at[place, f], at(fs=lax.rem(f + d, nf))
+        )
+
+    for core in range(2):
+
+        @pl.when(t == core)
+        def _(core=core):
+            for place in range(n):
+                part = wbuf.at[wrows(place, f), wcols(core)]
+                pltpu.make_async_copy(part, part, w_recv.at[place]).wait()
+                for d in range(1, nf):
+                    share(core, place, d).start()
+
+    for d in range(1, n):
+
+        @pl.when(s >= d)
+        def _(d=d):
+            place = s - d
+            token_right(place).wait_recv()
+            token_partner(place).start()
+
+            @pl.when(s < n - 1)
+            def _():
+                token_right(place).start()
+
+        @pl.when(s + d < n)
+        def _(d=d):
+            place = s + d
+            token_left(place).wait_recv()
+            token_partner(place).start()
+
+            @pl.when(s > 0)
+            def _():
+                token_left(place).start()
+
+    for place in range(n):
+        part = x.at[slot(place, other)]
+        remote(part, part, d_send.at[place], t_recv.at[place, other], at(tp=other)).wait_recv()
+    for core in range(2):
+
+        @pl.when(t == core)
+        def _(core=core):
+            for place in range(n):
+                for d in range(1, nf):
+                    quarter = lax.rem(f + d, nf)
+                    part = wbuf.at[wrows(place, quarter), wcols(core)]
+                    remote(
+                        part, part, x_send.at[place, d], x_recv.at[place, quarter], at(fs=quarter)
+                    ).wait_recv()
+
+    pltpu.make_async_copy(pk, pk, p_recv).wait()
+
+    total = x.shape[0]
+    chunk = min(256, total)
+
+    def project(core):
+        @pl.loop(0, total // chunk)
+        def _(i):
+            at_rows = pl.ds(pl.multiple_of(i * chunk, chunk), chunk)
+            proj[at_rows, wcols(core)] = jnp.dot(
+                x[at_rows, :], wbuf[:, wcols(core)], preferred_element_type=jnp.float32
+            ).astype(jnp.bfloat16)
+
+    def send_all(core, to_s, to_t):
+        dst = yall.at[:, pl.ds(pl.multiple_of(core * groups + s * width, width), width)]
+        return remote(
+            yout.at[to_t], dst, a_send.at[to_s, to_t], a_recv.at[s, core], at(sp=to_s, tp=to_t)
+        )
+
+    def spread(core):
+        for d in range(n):
+            for c in range(2):
+                if d or c:
+                    send_all(core, lax.rem(s + n - d, n), (core + c) % 2).start()
+        dst = yall.at[:, pl.ds(pl.multiple_of(core * groups + s * width, width), width)]
+        pltpu.make_async_copy(yout.at[core], dst, a_recv.at[s, core]).start()
+
+    def spread_wait(core):
+        for d in range(n):
+            for c in range(2):
+                if d or c:
+                    send_all(core, lax.rem(s + n - d, n), (core + c) % 2).wait_send()
+
+    @pl.when(t == 0)
+    def _():
+        project(0)
+        for place in range(n):
+            pltpu.make_async_copy(ld.at[place], ld.at[place], l_recv.at[place]).wait()
+        pick = lax.broadcasted_iota(jnp.int32, (PACK, width), 0)
+        span = 2 * rows
+        for place in range(n):
+            for d in range(2):
+                dec[d, pl.ds(place * span, span), :] = dot_as(
+                    ld[place], (pick == d).astype(jnp.float32), 0, 0
+                )
+        row_i = lax.broadcasted_iota(jnp.int32, (BLOCK, BLOCK), 0)
+        col_i = lax.broadcasted_iota(jnp.int32, (BLOCK, BLOCK), 1)
+        masks = (row_i >= col_i, row_i <= col_i)
+        blocks = total // BLOCK
+
+        def one(d, p, state):
+            at_rows = pl.ds(pl.multiple_of(p * BLOCK, BLOCK), BLOCK)
+            qp = proj[at_rows, 0:width].astype(jnp.float32)
+            query = qp * jax.nn.sigmoid(qp) * width ** (-0.5)
+            value = proj[at_rows, width : 2 * width].astype(jnp.float32)
+            pre = proj[at_rows, (2 + d) * width : (3 + d) * width].astype(jnp.float32)
+            keys = pk[2 + d : 3 + d, :] * jax.nn.sigmoid(-pre)
+            gate = jnp.log1p(-keys) + dec[d, at_rows, :]
+            cum = dot_as(masks[d].astype(jnp.float32), gate, 1, 0)
+            query_g = query * jnp.exp(cum)
+            key_g = keys * jnp.exp(-cum)
+            scores = jnp.where(masks[d], dot_as(query_g, key_g, 1, 1), 0.0)
+            result = dot_as(scores, value, 1, 0) + dot_as(query_g, state, 1, 1)
+            last = cum[BLOCK - 1 : BLOCK, :] if d == 0 else cum[0:1, :]
+            weighted = keys * jnp.exp(last - cum)
+            state = state * jnp.exp(last) + dot_as(value, weighted, 0, 0)
+            (accf, accb)[d][at_rows, :] = result
+            return state
+
+        def step(i, states):
+            return one(0, i, states[0]), one(1, blocks - 1 - i, states[1])
+
+        zero = jnp.zeros((width, width), jnp.float32)
+        lax.fori_loop(0, blocks, step, (zero, zero))
+        for place in range(n):
+            for c in range(2):
+                at_rows = pl.ds((place * 2 + c) * rows, rows)
+                joined = accf[at_rows, :] + accb[at_rows, :]
+                joined = joined * lax.rsqrt(
+                    jnp.mean(joined * joined, axis=-1, keepdims=True) + EPS
+                )
+                yout[c, pl.ds(place * rows, rows), :] = (joined * pk[4:5, :]).astype(jnp.bfloat16)
+        spread(0)
+
+    @pl.when(t == 1)
+    def _():
+        project(1)
+        taps = pk.shape[0] - PACK
+        pad = 16
+        gp[0:pad, :] = jnp.zeros((pad, width), jnp.float32)
+        gp[pad + total : 2 * pad + total, :] = jnp.zeros((pad, width), jnp.float32)
+        value = proj[:, 0:width].astype(jnp.float32)
+        gate = proj[:, width : 2 * width].astype(jnp.float32)
+        gp[pad : pad + total, :] = (
+            (value * jax.nn.sigmoid(gate)).astype(jnp.bfloat16).astype(jnp.float32)
+        )
+        first = pad - taps_half(taps)
+
+        for b in range(total // rows):
+            acc = jnp.zeros((rows, width), jnp.float32)
+            for j in range(taps):
+                acc = acc + pk[PACK + j : PACK + j + 1, :] * gp[pl.ds(b * rows + first + j, rows), :]
+            accf[pl.ds(b * rows, rows), :] = acc
+        conv = accf[...]
+        ones = jnp.ones((8, width), jnp.float32)
+        st[s, 0] = dot_as(ones, conv, 1, 1)
+        st[s, 1] = dot_as(ones, conv * conv, 1, 1)
+
+        def stat(d):
+            return remote(
+                st.at[s], st.at[s], s_send.at[d], s_recv.at[s], at(sp=lax.rem(s + d, n))
+            )
+
+        for d in range(1, n):
+            stat(d).start()
+        for d in range(1, n):
+            place = lax.rem(s + d, n)
+            remote(st.at[place], st.at[place], s_send.at[d], s_recv.at[place], at(sp=place)).wait_recv()
+        stats = st[0]
+        for place in range(1, n):
+            stats = stats + st[place]
+        stats = stats / groups
+        mean_r = stats[0]
+        inv_r = lax.rsqrt(stats[1] - mean_r * mean_r + EPS)
+        eighth = jnp.full((8, width), 0.125, jnp.float32)
+        mean_c = dot_as(mean_r, eighth, 0, 0)
+        inv_c = dot_as(inv_r, eighth, 0, 0)
+        out = (accf[...] - mean_c) * inv_c * pk[5:6, :]
+        out = (out * jax.nn.sigmoid(out)).astype(jnp.bfloat16)
+        for place in range(n):
+            for c in range(2):
+                b = (place * 2 + c) * rows
+                yout[c, pl.ds(place * rows, rows), :] = out[b : b + rows]
+        spread(1)
+        for d in range(1, n):
+            stat(d).wait_send()
+
+    for which, ref in enumerate((out_r, out_c)):
+        part = ow.at[pl.ds(pl.multiple_of(which * groups + t * half, half), half)]
+        pltpu.make_async_copy(ref, part, loc.at[which]).wait()
+        part = ow.at[pl.ds(pl.multiple_of(which * groups + other * half, half), half)]
+        remote(ref, part, o_send.at[which], o_recv.at[which], at(tp=other)).wait_recv()
+    for core in range(2):
+        for place in range(n):
+            part = yall.at[:, pl.ds(core * groups + place * width, width)]
+            pltpu.make_async_copy(part, part, a_recv.at[place, core]).wait()
+    result = jnp.dot(yall[...], ow[...], preferred_element_type=jnp.float32)
+    mo[...] = result.astype(jnp.bfloat16)
+    cols = out_r.shape[1]
+    fin_cols = pl.ds(pl.multiple_of(s * cols, cols), cols)
+
+    def give(to_s):
+        return remote(
+            mo.at[pl.ds(pl.multiple_of(to_s * rows, rows), rows)], fin.at[:, fin_cols],
+            f_send.at[to_s], f_recv.at[s], at(sp=to_s),
+        )
+
+    for d in range(1, n):
+        give(lax.rem(s + d, n)).start()
+    o_ref[0, :, fin_cols] = mo[pl.ds(pl.multiple_of(s * rows, rows), rows), :]
+    for d in range(1, n):
+        place = lax.rem(s + d, n)
+        part_cols = pl.ds(pl.multiple_of(place * cols, cols), cols)
+        remote(
+            mo.at[pl.ds(0, rows)], fin.at[:, part_cols], f_send.at[place], f_recv.at[place],
+            at(sp=place),
+        ).wait_recv()
+        o_ref[0, :, part_cols] = fin[:, part_cols]
+
+    for core in range(2):
+
+        @pl.when(t == core)
+        def _(core=core):
+            spread_wait(core)
+            for place in range(n):
+                for d in range(1, nf):
+                    share(core, place, d).wait_send()
+
+    for d in range(1, n):
+        give(lax.rem(s + d, n)).wait_send()
+    for copy in own_out:
+        copy.wait_send()
+    for j in range(hl):
+        to_s = t * hl + j
+        for core in range(2):
+
+            @pl.when(jnp.logical_not((to_s == s) & (t == core)))
+            def _(j=j, core=core, to_s=to_s):
+                part = wbuf.at[wrows(s, f), wcols(core)]
+                remote(
+                    part, part, w_send.at[j, core], w_recv.at[s], at(sp=to_s, tp=core)
+                ).wait_send()
+
+        @pl.when(jnp.logical_not((to_s == s) & (t == 0)))
+        def _(j=j, to_s=to_s):
+            remote(
+                pack.at[j, pl.ds(0, PACK)], ld.at[s], l_send.at[j], l_recv.at[s],
+                at(sp=to_s, tp=0),
+            ).wait_send()
+
+        @pl.when(to_s == s)
+        def _(j=j):
+            remote(pack.at[j], pk, p_send, p_recv, at(tp=other)).wait_send()
+
+    for place in range(n):
+        token_partner(place).wait_send()
+
+        @pl.when((place <= s) & (s < n - 1))
+        def _(place=place):
+            token_right(place).wait_send()
+
+        @pl.when((place >= s) & (s > 0))
+        def _(place=place):
+            token_left(place).wait_send()
+
+
+def taps_half(taps):
+    return taps // 2
+
+
+def fused_body(
+    n, nf, tokens, norm_gain, rec_query, rec_input, rec_forward, rec_backward, forget_gap,
+    log_decay, rec_gain, conv_value, conv_gate, conv_kernel, conv_gain, out_rec, out_conv,
+):
+    hl = log_decay.shape[2]
+    rows, d = tokens.shape[1:]
+    total = 2 * rows * n
+    taps = conv_kernel.shape[0]
+    width = KD
+    groups = n * width
+    cols = out_rec.shape[1]
+
+    def by_head(a):
+        return a.astype(jnp.float32).reshape(-1, hl, width).transpose(1, 0, 2)
+
+    pack = jnp.concatenate(
+        [
+            log_decay[0].transpose(1, 0, 2),
+            by_head(forget_gap),
+            by_head(rec_gain),
+            by_head(conv_gain),
+            jnp.zeros((hl, PACK - 6, width), jnp.float32),
+            by_head(conv_kernel),
+        ],
+        axis=1,
+    )
+    vmem = pl.BlockSpec(memory_space=pltpu.VMEM)
+    bf, f32 = jnp.bfloat16, jnp.float32
+    dma = pltpu.SemaphoreType.DMA
+    scratch = [
+        pltpu.VMEM((total, d), bf),
+        pltpu.VMEM((d, 4 * width), bf),
+        pltpu.VMEM((2 * groups, cols), bf),
+        pltpu.VMEM((PACK + taps, width), f32),
+        pltpu.VMEM((n, PACK, width), f32),
+        pltpu.VMEM((2, total, width), f32),
+        pltpu.VMEM((total, 4 * width), bf),
+        pltpu.VMEM((total, width), f32),
+        pltpu.VMEM((total, width), f32),
+        pltpu.VMEM((total + 32, width), f32),
+        pltpu.VMEM((2, total // 2, width), bf),
+        pltpu.VMEM((total // 2, 2 * groups), bf),
+        pltpu.VMEM((total // 2, cols), bf),
+        pltpu.VMEM((rows, d), bf),
+        pltpu.VMEM((n, 2, 8, total), f32),
+        dma((hl, 2)), dma((n,)),
+        dma((n, nf)), dma((n, nf)),
+        dma((n, 2)), dma((n, 2)), dma((n,)),
+        dma(()), dma(()),
+        dma((hl,)), dma((n,)),
+        dma((2,)), dma((2,)),
+        dma((n, 2)), dma((n, 2)),
+        dma((n,)), dma((n,)),
+        dma((n,)), dma((n,)),
+        dma((2,)),
+    ]
+    return pl.pallas_call(
+        functools.partial(fused_kernel, n, nf, hl),
+        out_shape=jax.ShapeDtypeStruct((1, rows, d), bf),
+        in_specs=[vmem] * 11,
+        out_specs=vmem,
+        scratch_shapes=scratch,
+        compiler_params=pltpu.CompilerParams(
+            collective_id=0, has_side_effects=True, vmem_limit_bytes=40 * 1024 * 1024
+        ),
+    )(
+        tokens, norm_gain[None], rec_query, rec_input, rec_forward, rec_backward, conv_value,
+        conv_gate, pack, out_rec, out_conv,
+    )
+
+
+def fits(n, nf, nt, tokens, rec_query, log_decay, conv_value, conv_kernel, out_rec):
+    heads = log_decay.shape[2]
+    rows = tokens.shape[1] // (n * nt)
+    return (
+        nt == 2
+        and n == heads
+        and tokens.shape[0] == nf
+        and rec_query.shape[1] == heads * KD
+        and conv_value.shape[1] == heads * VD
+        and KD == VD
+        and 2 * rows == KD
+        and rec_query.shape[0] % (n * nf * 16) == 0
+        and conv_kernel.shape[0] // 2 <= 15
+    )
+
+
+def layer(mesh, *args):
+    n, nf, nt = (mesh.shape[a] for a in ("sp", "fs", "tp"))
+    fast = fits(n, nf, nt, args[0], args[2], args[7], args[9], args[11], args[13])
+    return sharded(mesh, functools.partial(fused_body, n, nf) if fast else body)(*args)
+
+
 def solution(mesh):
+    return functools.partial(layer, mesh)
+
+
+def sharded(mesh, body):
     return jax.shard_map(
         body,
         mesh=mesh,

time: 255 us -> 73.6 us (0.29)
  waiting for transfers between devices: 153 us -> 0 us
  Pallas kernels: 0 us -> 60.9 us
  blocking collectives: 57.2 us -> 0 us
  matrix products: 19.5 us -> 0 us
  between operations: 13.9 us -> 0.07 us
  local copies, waits for them, and re-layouts: 0.98 us -> 12.1 us
  starting transfers between devices: 4.92 us -> 0 us
  other arithmetic: 3.83 us -> 0 us
    all_gather x7 -> x0, waiting for transfers between devices: 143 us -> none  [the longest x1 27.4 us: body(): lax.all_gather(rec_forward, 'sp', axis=0, tiled=True)]
    pallas_call x0 -> x1, Pallas kernels: none -> 60.9 us  [fused_body(): pl.pallas_call(functools.partial(fused_kernel, n, nf, hl), out_shape=jax....]
    all_gather x5 -> x0, blocking collectives: 54.7 us -> none  [the longest x4 52.4 us: entering(): lax.all_gather(a.astype(kind), axis)]
    dot_general x25 -> x0, matrix products: 17.3 us -> none  [the longest x6 9.23 us: body(): jnp.dot(whole, weight_piece, preferred_element_type=jnp.float32)]
    unnamed x14 -> x30, local copies, waits for them, and re-layouts: 0.03 us -> 11.3 us
    reduce_scatter x1 -> x0, waiting for transfers between devices: 6.88 us -> none  [body(): lax.psum_scatter(jnp.dot(rows_part, full_columns, preferred_element_type=...]
    ppermute x2 -> x0, starting transfers between devices: 4.65 us -> none  [the longest x1 3.35 us: padded_2(): lax.ppermute(tail, axis, [(i, (i + 1) % count) for i in range(ends)])]
    unnamed x8 -> x0, waiting for transfers between devices: 3.7 us -> none
  transfers between devices with their start and end apart: 10 -> 0, of which waited for: 7 -> 0; matrix products, arithmetic and copies ran while one was open for 8% -> 0% of each run, Pallas kernels for 0% -> 0%
where the time goes in v1:
time: 73.6 us; the launch traced here: 73 us
  Pallas kernels  60.9 us (83%)
  local copies, waits for them, and re-layouts  12.1 us (16%)
    pallas_call x1, Pallas kernels, fused_body(): pl.pallas_call(functools.partial(fused_kernel, n, nf, hl), out_shape=jax....  60.9 us
    unnamed x30, local copies, waits for them, and re-layouts  11.3 us

profile of v1, /device:TPU:0, one launch (start us, length us, event | category | flops | bytes accessed | tf_op | source)
XLA Modules:
  0.0 73.0 jit_solution(2923904345765777977)
XLA Ops:
  0.0 0.0 copy-start.11
  0.0 0.7 copy-done.11
  0.7 0.7 %reshape.9 = f32[31,2,128]{2,1,0:T(2,128)S(1)} reshape(bf16[31,256]{1,0:T(8,128)(2,1)} %param.26) | data formatting | bytes 47616 | tf_op jit(solution)/shard_map/transpose | solution.py:640
  1.4 0.0 copy-start.10
  1.4 0.0 copy-start.12
  1.5 0.0 copy-start.13
  1.5 0.6 copy-done.10
  2.1 0.0 copy-done.12
  2.1 0.0 copy-done.13
  2.2 0.0 copy-start.9
  2.2 0.7 copy-done.9
  2.8 0.0 copy-start
  2.9 0.9 %copy-done = bf16[1,64,2048]{2,1,0:T(8,128)(2,1)S(1)} copy-done((bf16[1,64,2048]{2,1,0:T(8,128)(2,1)S(1)}, bf16[1,64,2048]{2,1,0:T(8,128)(2,1)}, u32[]{:S(2)}) %copy-start) | copy-done | bytes 262168
  3.8 0.0 copy-start.1
  3.8 0.9 %copy-done.1 = bf16[512,256]{1,0:T(8,128)(2,1)S(1)} copy-done((bf16[512,256]{1,0:T(8,128)(2,1)S(1)}, bf16[512,256]{1,0:T(8,128)(2,1)}, u32[]{:S(2)}) %copy-start.1) | copy-done | bytes 262168
  4.8 0.0 copy-start.2
  4.8 0.9 %copy-done.2 = bf16[512,256]{1,0:T(8,128)(2,1)S(1)} copy-done((bf16[512,256]{1,0:T(8,128)(2,1)S(1)}, bf16[512,256]{1,0:T(8,128)(2,1)}, u32[]{:S(2)}) %copy-start.2) | copy-done | bytes 262168
  5.7 0.0 copy-start.3
  5.7 0.9 %copy-done.3 = bf16[512,256]{1,0:T(8,128)(2,1)S(1)} copy-done((bf16[512,256]{1,0:T(8,128)(2,1)S(1)}, bf16[512,256]{1,0:T(8,128)(2,1)}, u32[]{:S(2)}) %copy-start.3) | copy-done | bytes 262168
  6.7 0.0 copy-start.4
  6.7 0.9 %copy-done.4 = bf16[512,256]{1,0:T(8,128)(2,1)S(1)} copy-done((bf16[512,256]{1,0:T(8,128)(2,1)S(1)}, bf16[512,256]{1,0:T(8,128)(2,1)}, u32[]{:S(2)}) %copy-start.4) | copy-done | bytes 262168
  7.6 0.0 copy-start.5
  7.6 0.9 %copy-done.5 = bf16[512,256]{1,0:T(8,128)(2,1)S(1)} copy-done((bf16[512,256]{1,0:T(8,128)(2,1)S(1)}, bf16[512,256]{1,0:T(8,128)(2,1)}, u32[]{:S(2)}) %copy-start.5) | copy-done | bytes 262168
  8.6 0.0 copy-start.6
  8.6 0.9 %copy-done.6 = bf16[512,256]{1,0:T(8,128)(2,1)S(1)} copy-done((bf16[512,256]{1,0:T(8,128)(2,1)S(1)}, bf16[512,256]{1,0:T(8,128)(2,1)}, u32[]{:S(2)}) %copy-start.6) | copy-done | bytes 262168
  9.5 0.0 copy-start.7
  9.5 0.9 %copy-done.7 = bf16[256,512]{1,0:T(8,128)(2,1)S(1)} copy-done((bf16[256,512]{1,0:T(8,128)(2,1)S(1)}, bf16[256,512]{1,0:T(8,128)(2,1)}, u32[]{:S(2)}) %copy-start.7) | copy-done | bytes 262168
  10.5 0.0 copy-start.8
  10.5 0.9 %copy-done.8 = bf16[256,512]{1,0:T(8,128)(2,1)S(1)} copy-done((bf16[256,512]{1,0:T(8,128)(2,1)S(1)}, bf16[256,512]{1,0:T(8,128)(2,1)}, u32[]{:S(2)}) %copy-start.8) | copy-done | bytes 262168
  11.4 60.9 %shard_map.145 = bf16[1,64,2048]{2,1,0:T(8,128)(2,1)S(1)} custom-call(bf16[1,64,2048]{2,1,0:T(8,128)(2,1)S(1)} %copy-done, f32[1,2048]{1,0:T(1,128)S(1)} %bitcast.14, bf16[512,256]{1,0:T(8,128)(2,1)S(1)} %copy-done.1, bf16[512,256]{1,0:T(8,128)(2,1)S(1)} %copy-done.2, bf16[512,256]{1,0:T(8,128)(2,1)S(1)} %copy-done.3, bf16[512,256]{1,0:T(8,128)(2,1)S(1)} %copy-done.4, ...), custom_call_target="tpu_custom_call" | custom-call | tf_op jit(solution)/shard_map/pallas_call | solution.py:683
  72.3 0.7 copy.24
  (4 shorter events, 0.0 us)
Async XLA Ops:
  0.0 0.7 copy-start.11
  1.4 0.7 copy-start.10
  1.4 0.7 copy-start.12
  1.5 0.7 copy-start.13
  2.2 0.7 copy-start.9
  2.8 0.9 %copy-start = (bf16[1,64,2048]{2,1,0:T(8,128)(2,1)S(1)}, bf16[1,64,2048]{2,1,0:T(8,128)(2,1)}, u32[]{:S(2)}) copy-start(bf16[1,64,2048]{2,1,0:T(8,128)(2,1)} %tokens.1) | copy-start | bytes 786436
  3.8 0.9 %copy-start.1 = (bf16[512,256]{1,0:T(8,128)(2,1)S(1)}, bf16[512,256]{1,0:T(8,128)(2,1)}, u32[]{:S(2)}) copy-start(bf16[512,256]{1,0:T(8,128)(2,1)} %w0.1) | copy-start | bytes 786436
  4.8 0.9 %copy-start.2 = (bf16[512,256]{1,0:T(8,128)(2,1)S(1)}, bf16[512,256]{1,0:T(8,128)(2,1)}, u32[]{:S(2)}) copy-start(bf16[512,256]{1,0:T(8,128)(2,1)} %w1.1) | copy-start | bytes 786436
  5.7 0.9 %copy-start.3 = (bf16[512,256]{1,0:T(8,128)(2,1)S(1)}, bf16[512,256]{1,0:T(8,128)(2,1)}, u32[]{:S(2)}) copy-start(bf16[512,256]{1,0:T(8,128)(2,1)} %w2.1) | copy-start | bytes 786436
  6.7 0.9 %copy-start.4 = (bf16[512,256]{1,0:T(8,128)(2,1)S(1)}, bf16[512,256]{1,0:T(8,128)(2,1)}, u32[]{:S(2)}) copy-start(bf16[512,256]{1,0:T(8,128)(2,1)} %w3.1) | copy-start | bytes 786436
  7.6 0.9 %copy-start.5 = (bf16[512,256]{1,0:T(8,128)(2,1)S(1)}, bf16[512,256]{1,0:T(8,128)(2,1)}, u32[]{:S(2)}) copy-start(bf16[512,256]{1,0:T(8,128)(2,1)} %w4.1) | copy-start | bytes 786436
  8.6 0.9 %copy-start.6 = (bf16[512,256]{1,0:T(8,128)(2,1)S(1)}, bf16[512,256]{1,0:T(8,128)(2,1)}, u32[]{:S(2)}) copy-start(bf16[512,256]{1,0:T(8,128)(2,1)} %w5.1) | copy-start | bytes 786436
  9.5 0.9 %copy-start.7 = (bf16[256,512]{1,0:T(8,128)(2,1)S(1)}, bf16[256,512]{1,0:T(8,128)(2,1)}, u32[]{:S(2)}) copy-start(bf16[256,512]{1,0:T(8,128)(2,1)} %out_r.1) | copy-start | bytes 786436
  10.5 0.9 %copy-start.8 = (bf16[256,512]{1,0:T(8,128)(2,1)S(1)}, bf16[256,512]{1,0:T(8,128)(2,1)}, u32[]{:S(2)}) copy-start(bf16[256,512]{1,0:T(8,128)(2,1)} %out_c.1) | copy-start | bytes 786436

commit v2 on v1

--- a/solution.py
+++ b/solution.py
@@ -231,10 +231,11 @@
 
 
 def fused_kernel(
-    n, nf, hl, tokens, gain, w0, w1, w2, w3, w4, w5, pack, out_r, out_c, o_ref,
-    x, wbuf, ow, pk, ld, dec, proj, accf, accb, gp, yout, yall, mo, fin, st,
+    n, nf, hl, tokens_in, gain_in, w0, w1, w2, w3, w4, w5, decay_in, gap_in,
+    rgain_in, cgain_in, taps_in, out_r, out_c, o_ref, decay_v, gap_v, rgain_v, cgain_v, taps_v,
+    tokens, gain, pack,    x, wbuf, ow, pk, ld, dec, proj, accf, accb, gp, yout, yall, mo, fin, st,
     w_send, w_recv, x_send, x_recv, t_send, t_recv, d_send, p_send, p_recv, l_send, l_recv,
-    o_send, o_recv, a_send, a_recv, f_send, f_recv, s_send, s_recv, loc,
+    o_send, o_recv, a_send, a_recv, f_send, f_recv, s_send, s_recv, loc, ini,
 ):
     s = lax.axis_index("sp")
     f = lax.axis_index("fs")
@@ -257,6 +258,18 @@
             device_id_type=MESH,
         )
 
+    entry = [
+        pltpu.make_async_copy(src, dst, ini.at[i])
+        for i, (src, dst) in enumerate(
+            (
+                (tokens_in, tokens), (gain_in, gain), (decay_in, decay_v), (gap_in, gap_v),
+                (rgain_in, rgain_v), (cgain_in, cgain_v), (taps_in, taps_v),
+            )
+        )
+    ]
+    for copy in entry:
+        copy.start()
+
     barrier = pltpu.get_barrier_semaphore()
     for d in range(n):
         for c in range(2):
@@ -277,26 +290,80 @@
     def wcols(core):
         return pl.ds(0, (4 - 2 * core) * width)
 
+    def whole(place):
+        return pl.ds(pl.multiple_of(place * kslice, kslice), kslice)
+
     mine = pl.ds(pl.multiple_of(f * krows, krows), krows)
     for j in range(hl):
         to_s = t * hl + j
         cols = pl.ds(j * width, width)
         for core in range(2):
-            here = (to_s == s) & (t == core)
             for at_m, m in enumerate((0, 1, 2, 3) if core == 0 else (4, 5)):
-                src = weights[m].at[mine, cols]
-                dst = wbuf.at[wrows(s, f), pl.ds(at_m * width, width)]
-
-                @pl.when(here)
+                at_cols = pl.ds(at_m * width, width)
+                src = weights[m].at[:, cols]
+                dst = wbuf.at[whole(s), at_cols]
+
+                @pl.when((to_s == s) & (t == core))
                 def _(src=src, dst=dst):
                     pltpu.make_async_copy(src, dst, w_recv.at[s]).start()
 
-                @pl.when(jnp.logical_not(here))
-                def _(src=src, dst=dst, core=core, to_s=to_s):
+                @pl.when((to_s == s) & (t != core))
+                def _(src=src, dst=dst, core=core, j=j):
+                    remote(src, dst, w_send.at[j, core], w_recv.at[s], at(tp=core)).start()
+
+                @pl.when(to_s != s)
+                def _(m=m, cols=cols, at_cols=at_cols, core=core, to_s=to_s, j=j):
                     remote(
-                        src, dst, w_send.at[j, core], w_recv.at[s], at(sp=to_s, tp=core)
+                        weights[m].at[mine, cols], wbuf.at[wrows(s, f), at_cols],
+                        w_send.at[j, core], w_recv.at[s], at(sp=to_s, tp=core),
                     ).start()
 
+    for copy in entry[2:]:
+        copy.wait()
+    taps_n = taps_v.shape[0]
+    for j in range(hl):
+        cols = slice(j * width, (j + 1) * width)
+        pack[j, 0:2, :] = decay_v[0, :, j, :]
+        pack[j, 2:4, :] = gap_v[:, cols]
+        pack[j, 4:5, :] = rgain_v[:, cols]
+        pack[j, 5:6, :] = cgain_v[:, cols]
+        pack[j, 6:PACK, :] = jnp.zeros((PACK - 6, width), jnp.float32)
+        pack[j, PACK : PACK + taps_n, :] = taps_v[:, cols].astype(jnp.float32)
+    entry[0].wait()
+    entry[1].wait()
+    values = tokens[0].astype(jnp.float32)
+    normed = values * lax.rsqrt(jnp.mean(values * values, axis=-1, keepdims=True) + EPS)
+
+    def slot(place, core):
+        return pl.ds(pl.multiple_of(place * 2 * rows + core * rows, rows), rows)
+
+    x[slot(s, t), :] = (normed * gain[...]).astype(jnp.bfloat16)
+
+    def token(place, core, send, to):
+        part = x.at[slot(place, core)]
+        return remote(part, part, send, t_recv.at[place, core], to)
+
+    def token_right(place):
+        return token(place, t, t_send.at[place, 0], at(sp=lax.rem(s + 1, n)))
+
+    def token_left(place):
+        return token(place, t, t_send.at[place, 1], at(sp=lax.rem(s + n - 1, n)))
+
+    def token_partner(place):
+        return token(place, t, d_send.at[place], at(tp=other))
+
+    @pl.when(s < n - 1)
+    def _():
+        token_right(s).start()
+
+    @pl.when(s > 0)
+    def _():
+        token_left(s).start()
+
+    token_partner(s).start()
+
+    for j in range(hl):
+        to_s = t * hl + j
         here0 = (to_s == s) & (t == 0)
         src = pack.at[j, pl.ds(0, PACK)]
 
@@ -312,37 +379,6 @@
         def _(j=j):
             pltpu.make_async_copy(pack.at[j], pk, p_recv).start()
             remote(pack.at[j], pk, p_send, p_recv, at(tp=other)).start()
-
-    values = tokens[0].astype(jnp.float32)
-    normed = values * lax.rsqrt(jnp.mean(values * values, axis=-1, keepdims=True) + EPS)
-
-    def slot(place, core):
-        return pl.ds(pl.multiple_of(place * 2 * rows + core * rows, rows), rows)
-
-    x[slot(s, t), :] = (normed * gain[...]).astype(jnp.bfloat16)
-
-    def token(place, core, send, to):
-        part = x.at[slot(place, core)]
-        return remote(part, part, send, t_recv.at[place, core], to)
-
-    def token_right(place):
-        return token(place, t, t_send.at[place, 0], at(sp=lax.rem(s + 1, n)))
-
-    def token_left(place):
-        return token(place, t, t_send.at[place, 1], at(sp=lax.rem(s + n - 1, n)))
-
-    def token_partner(place):
-        return token(place, t, d_send.at[place], at(tp=other))
-
-    @pl.when(s < n - 1)
-    def _():
-        token_right(s).start()
-
-    @pl.when(s > 0)
-    def _():
-        token_left(s).start()
-
-    token_partner(s).start()
 
     own_out = []
     for which, ref in enumerate((out_r, out_c)):
@@ -361,7 +397,8 @@
 
         @pl.when(t == core)
         def _(core=core):
-            for place in range(n):
+            for e in range(1, n):
+                place = lax.rem(s + e, n)
                 part = wbuf.at[wrows(place, f), wcols(core)]
                 pltpu.make_async_copy(part, part, w_recv.at[place]).wait()
                 for d in range(1, nf):
@@ -396,7 +433,10 @@
 
         @pl.when(t == core)
         def _(core=core):
-            for place in range(n):
+            part = wbuf.at[whole(s), wcols(core)]
+            pltpu.make_async_copy(part, part, w_recv.at[s]).wait()
+            for e in range(1, n):
+                place = lax.rem(s + e, n)
                 for d in range(1, nf):
                     quarter = lax.rem(f + d, nf)
                     part = wbuf.at[wrows(place, quarter), wcols(core)]
@@ -578,9 +618,9 @@
         @pl.when(t == core)
         def _(core=core):
             spread_wait(core)
-            for place in range(n):
+            for e in range(1, n):
                 for d in range(1, nf):
-                    share(core, place, d).wait_send()
+                    share(core, lax.rem(s + e, n), d).wait_send()
 
     for d in range(1, n):
         give(lax.rem(s + d, n)).wait_send()
@@ -590,7 +630,12 @@
         to_s = t * hl + j
         for core in range(2):
 
-            @pl.when(jnp.logical_not((to_s == s) & (t == core)))
+            @pl.when((to_s == s) & (t != core))
+            def _(j=j, core=core):
+                part = wbuf.at[whole(s), wcols(core)]
+                remote(part, part, w_send.at[j, core], w_recv.at[s], at(tp=core)).wait_send()
+
+            @pl.when(to_s != s)
             def _(j=j, core=core, to_s=to_s):
                 part = wbuf.at[wrows(s, f), wcols(core)]
                 remote(
@@ -636,24 +681,15 @@
     groups = n * width
     cols = out_rec.shape[1]
 
-    def by_head(a):
-        return a.astype(jnp.float32).reshape(-1, hl, width).transpose(1, 0, 2)
-
-    pack = jnp.concatenate(
-        [
-            log_decay[0].transpose(1, 0, 2),
-            by_head(forget_gap),
-            by_head(rec_gain),
-            by_head(conv_gain),
-            jnp.zeros((hl, PACK - 6, width), jnp.float32),
-            by_head(conv_kernel),
-        ],
-        axis=1,
-    )
     vmem = pl.BlockSpec(memory_space=pltpu.VMEM)
     bf, f32 = jnp.bfloat16, jnp.float32
     dma = pltpu.SemaphoreType.DMA
+    small = (log_decay, forget_gap, rec_gain[None], conv_gain[None], conv_kernel)
     scratch = [
+        *(pltpu.VMEM(a.shape, a.dtype) for a in small),
+        pltpu.VMEM(tokens.shape, bf),
+        pltpu.VMEM((1, d), f32),
+        pltpu.VMEM((hl, PACK + taps, width), f32),
         pltpu.VMEM((total, d), bf),
         pltpu.VMEM((d, 4 * width), bf),
         pltpu.VMEM((2 * groups, cols), bf),
@@ -678,20 +714,20 @@
         dma((n, 2)), dma((n, 2)),
         dma((n,)), dma((n,)),
         dma((n,)), dma((n,)),
-        dma((2,)),
+        dma((2,)), dma((7,)),
     ]
     return pl.pallas_call(
         functools.partial(fused_kernel, n, nf, hl),
         out_shape=jax.ShapeDtypeStruct((1, rows, d), bf),
-        in_specs=[vmem] * 11,
+        in_specs=[pl.BlockSpec(memory_space=pl.ANY)] * 15,
         out_specs=vmem,
         scratch_shapes=scratch,
         compiler_params=pltpu.CompilerParams(
-            collective_id=0, has_side_effects=True, vmem_limit_bytes=40 * 1024 * 1024
+            collective_id=0, has_side_effects=True, vmem_limit_bytes=60 * 1024 * 1024
         ),
     )(
         tokens, norm_gain[None], rec_query, rec_input, rec_forward, rec_backward, conv_value,
-        conv_gate, pack, out_rec, out_conv,
+        conv_gate, *small, out_rec, out_conv,
     )
 
 

time: 73.6 us -> 62.8 us (0.85)
  local copies, waits for them, and re-layouts: 12.1 us -> 1.67 us
    unnamed x30 -> x1, local copies, waits for them, and re-layouts: 11.3 us -> 1.67 us
    pallas_call x1, Pallas kernels: 60.9 us -> 60.2 us  [fused_body(): pl.pallas_call(functools.partial(fused_kernel, n, nf, hl), out_shape=jax....]
    transpose x2 -> x0, local copies, waits for them, and re-layouts: 0.74 us -> none  [by_head(): return a.astype(jnp.float32).reshape(-1, hl, width).transpose(1, 0, 2)]
where the time goes in v2:
time: 62.8 us; the launch traced here: 61.9 us
  Pallas kernels  60.2 us (96%)
  local copies, waits for them, and re-layouts  1.67 us (3%)
    pallas_call x1, Pallas kernels, fused_body(): pl.pallas_call(functools.partial(fused_kernel, n, nf, hl), out_shape=jax....  60.2 us
    unnamed x1, local copies, waits for them, and re-layouts  1.67 us

profile of v2, /device:TPU:0, one launch (start us, length us, event | category | flops | bytes accessed | tf_op | source)
XLA Modules:
  0.0 61.9 jit_solution(12840744761778568382)
XLA Ops:
  0.0 60.2 %shard_map.145 = bf16[1,64,2048]{2,1,0:T(8,128)(2,1)} custom-call(bf16[1,64,2048]{2,1,0:T(8,128)(2,1)} %tokens_in.1, f32[1,2048]{1,0:T(1,128)} %bitcast.3, bf16[512,256]{1,0:T(8,128)(2,1)} %w0.1, bf16[512,256]{1,0:T(8,128)(2,1)} %w1.1, bf16[512,256]{1,0:T(8,128)(2,1)} %w2.1, bf16[512,256]{1,0:T(8,128)(2,1)} %w3.1, bf16[512,256]{1,0:T(8,128)(2,1)} %w4.1, ...), custom_call_target="tpu_custom_call" | custom-call | tf_op jit(solution)/shard_map/pallas_call | solution.py:719
  60.2 1.7 %copy.17 = bf16[1,64,2048]{2,1,0:T(8,128)(2,1)} copy(bf16[1,64,2048]{2,1,0:T(8,128)(2,1)} %shard_map.145) | data formatting | bytes 524288

commit v3 on v2

--- a/solution.py
+++ b/solution.py
@@ -230,6 +230,20 @@
     )
 
 
+def dot_exact(a, b, ca, cb, split):
+    parts = [a, b]
+    left = parts[split]
+    parts[1 - split] = parts[1 - split].astype(jnp.bfloat16)
+    total = None
+    for _ in range(3):
+        piece = left.astype(jnp.bfloat16)
+        left = left - piece.astype(jnp.float32)
+        parts[split] = piece
+        term = dot_as(parts[0], parts[1], ca, cb, lax.Precision.DEFAULT)
+        total = term if total is None else total + term
+    return total
+
+
 def fused_kernel(
     n, nf, hl, tokens_in, gain_in, w0, w1, w2, w3, w4, w5, decay_in, gap_in,
     rgain_in, cgain_in, taps_in, out_r, out_c, o_ref, decay_v, gap_v, rgain_v, cgain_v, taps_v,
@@ -502,7 +516,7 @@
             pre = proj[at_rows, (2 + d) * width : (3 + d) * width].astype(jnp.float32)
             keys = pk[2 + d : 3 + d, :] * jax.nn.sigmoid(-pre)
             gate = jnp.log1p(-keys) + dec[d, at_rows, :]
-            cum = dot_as(masks[d].astype(jnp.float32), gate, 1, 0)
+            cum = dot_exact(masks[d].astype(jnp.float32), gate, 1, 0, 1)
             query_g = query * jnp.exp(cum)
             key_g = keys * jnp.exp(-cum)
             scores = jnp.where(masks[d], dot_as(query_g, key_g, 1, 1), 0.0)
@@ -549,8 +563,8 @@
             accf[pl.ds(b * rows, rows), :] = acc
         conv = accf[...]
         ones = jnp.ones((8, width), jnp.float32)
-        st[s, 0] = dot_as(ones, conv, 1, 1)
-        st[s, 1] = dot_as(ones, conv * conv, 1, 1)
+        st[s, 0] = dot_exact(ones, conv, 1, 1, 1)
+        st[s, 1] = dot_exact(ones, conv * conv, 1, 1, 1)
 
         def stat(d):
             return remote(
@@ -569,8 +583,8 @@
         mean_r = stats[0]
         inv_r = lax.rsqrt(stats[1] - mean_r * mean_r + EPS)
         eighth = jnp.full((8, width), 0.125, jnp.float32)
-        mean_c = dot_as(mean_r, eighth, 0, 0)
-        inv_c = dot_as(inv_r, eighth, 0, 0)
+        mean_c = dot_exact(mean_r, eighth, 0, 0, 0)
+        inv_c = dot_exact(inv_r, eighth, 0, 0, 0)
         out = (accf[...] - mean_c) * inv_c * pk[5:6, :]
         out = (out * jax.nn.sigmoid(out)).astype(jnp.bfloat16)
         for place in range(n):

time: 62.8 us -> 63.1 us (level); the launches traced: 61.9 us -> 62.9 us
  Pallas kernels: 60.2 us -> 61.2 us
    pallas_call x1, Pallas kernels: 60.2 us -> 61.2 us  [fused_body(): pl.pallas_call(functools.partial(fused_kernel, n, nf, hl), out_shape=jax....]
where the time goes in v3:
time: 63.1 us; the launch traced here: 62.9 us
  Pallas kernels  61.2 us (97%)
  local copies, waits for them, and re-layouts  1.67 us (3%)
    pallas_call x1, Pallas kernels, fused_body(): pl.pallas_call(functools.partial(fused_kernel, n, nf, hl), out_shape=jax....  61.2 us
    unnamed x1, local copies, waits for them, and re-layouts  1.67 us

profile of v3, /device:TPU:0, one launch (start us, length us, event | category | flops | bytes accessed | tf_op | source)
XLA Modules:
  0.0 62.9 jit_solution(16817904711523535)
XLA Ops:
  0.0 61.2 %shard_map.145 = bf16[1,64,2048]{2,1,0:T(8,128)(2,1)} custom-call(bf16[1,64,2048]{2,1,0:T(8,128)(2,1)} %tokens_in.1, f32[1,2048]{1,0:T(1,128)} %bitcast.3, bf16[512,256]{1,0:T(8,128)(2,1)} %w0.1, bf16[512,256]{1,0:T(8,128)(2,1)} %w1.1, bf16[512,256]{1,0:T(8,128)(2,1)} %w2.1, bf16[512,256]{1,0:T(8,128)(2,1)} %w3.1, bf16[512,256]{1,0:T(8,128)(2,1)} %w4.1, ...), custom_call_target="tpu_custom_call" | custom-call | tf_op jit(solution)/shard_map/pallas_call | solution.py:733
  61.3 1.7 %copy.17 = bf16[1,64,2048]{2,1,0:T(8,128)(2,1)} copy(bf16[1,64,2048]{2,1,0:T(8,128)(2,1)} %shard_map.145) | data formatting | bytes 524288
